TPU v7x, 32 devices: a whole 2x2x4 slice. The times are simulated.
32 devices in a mesh: sp: 8 (over z, y), tp: 4 (over x, core).
Axes of the slice: x: 2, y: 2, z: 4, core: 2. Of those that a mesh axis runs over, the one named last changes fastest.
Arguments:
- tokens: bfloat16 [2048, 2048], P(('sp', 'tp')), may hold values from -6 to 6
- norm_gain: float32 [2048], replicated, may hold values from 0.1 to 6, as said below
- query_weight: bfloat16 [2048, 16, 128], P(None, 'tp'), may hold values from -0.21875 to 0.21875
- key_weight: bfloat16 [2048, 4, 128], P(None, 'tp'), may hold values from -0.125 to 0.125
- value_weight: bfloat16 [2048, 4, 128], P(None, 'tp'), may hold values from -0.125 to 0.125
- mix_lambda: float32 [16], P('tp'), may hold values from 0.3 to 0.8
- head_gain: float32 [128], replicated, may hold values from 0.1 to 1.9
- pool_weight: bfloat16 [2048, 4, 512], P(None, 'tp'), may hold values from -0.125 to 0.125
- pool_mix: bfloat16 [4, 512, 512], P('tp'), may hold values from -0.25 to 0.25
- pool_scale: float32 [4, 512], P('tp'), may hold values from 0.1 to 1.9
- gate_weight: bfloat16 [2048, 2, 2048], P(None, None, 'tp'), may hold values from -0.125 to 0.125
- out_weight: bfloat16 [2048, 2048], P('tp'), may hold values from -0.125 to 0.125
Outputs:
- mixed: bfloat16 [2048, 2048], P(('sp', 'tp'))
- log_sums: float32 [2, 16, 2048], P(None, 'tp', 'sp')
Inputs may be any that keep to these rules, and one draw needn't show every extreme that they name: `norm_gain`: positive.
All inputs are finite; a program needn't handle non-finite values.
Results may differ from a plain program's by a relative error of at most 0.013.
Values may be sent and summed in bfloat16 or wider, within the bound.
A program may use at most 128 MiB of HBM per device.

v0:
```python
import math

import jax
import jax.numpy as jnp
from jax import lax
from jax.sharding import PartitionSpec as P

WINDOW = 16


NORM_EPS = 1e-06


def shifted(block, axis, distance):
    devices = range(lax.axis_size(axis))
    route = [(i - distance, i) for i in devices if i - distance in devices]
    return lax.ppermute(block, axis, route)


def attend(
    queries, key_buffer, value_buffer, key_start, query_start, weight_lambda, head_dim, value_dim
):
    tok_rows, kv_local, group_size = (queries.shape[0], queries.shape[1], queries.shape[2])
    total_keys = key_buffer.shape[0]
    block_keys = math.gcd(total_keys, 512)
    keys_split = key_buffer.reshape(total_keys, kv_local, 2, head_dim)
    values_split = value_buffer.reshape(total_keys, kv_local, value_dim)
    query_pos = query_start + jnp.arange(tok_rows, dtype=jnp.int32)
    score_scale = head_dim ** (-0.5)
    low_index = jnp.maximum(0, -key_start)
    high_index = query_start + tok_rows - key_start
    first_block = low_index // block_keys
    last_block = (high_index + block_keys - 1) // block_keys

    def online_step(block_index, carry):
        running_max, running_sum, accum = carry
        key_begin = block_index * block_keys
        block_keys_arr = lax.dynamic_slice_in_dim(keys_split, key_begin, block_keys, 0)
        scores = (
            jnp.einsum(
                "qgrmd,kgmd->grmqk", queries, block_keys_arr, preferred_element_type=jnp.float32
            )
            * score_scale
        )
        key_pos = key_start + key_begin + jnp.arange(block_keys, dtype=jnp.int32)
        visible = (key_pos[None, :] <= query_pos[:, None]) & (key_pos[None, :] >= 0)
        block_max = jnp.max(jnp.where(visible, scores, -1e30), axis=4)
        new_max = jnp.maximum(running_max, block_max)
        rescale = jnp.exp(running_max - new_max)
        probs = jnp.where(visible, jnp.exp(scores - new_max[..., None]), 0.0)
        new_sum = running_sum * rescale + jnp.sum(probs, axis=4)
        block_values = lax.dynamic_slice_in_dim(values_split, key_begin, block_keys, 0)
        new_accum = accum * rescale[..., None] + jnp.einsum(
            "grmqk,kgd->grmqd",
            probs.astype(jnp.bfloat16),
            block_values,
            preferred_element_type=jnp.float32,
        )
        return (new_max, new_sum, new_accum)

    start_carry = (
        jnp.full((kv_local, group_size, 2, tok_rows), -1e30, jnp.float32),
        jnp.zeros((kv_local, group_size, 2, tok_rows), jnp.float32),
        jnp.zeros((kv_local, group_size, 2, tok_rows, value_dim), jnp.float32),
    )
    running_max, running_sum, accum = lax.fori_loop(
        first_block, last_block, online_step, start_carry
    )
    first_map = accum[:, :, 0] / running_sum[:, :, 0, :, None]
    second_map = accum[:, :, 1] / running_sum[:, :, 1, :, None]
    head_out = first_map - weight_lambda[:, :, None, None] * second_map
    log_sums = running_max + jnp.log(running_sum)
    return (head_out, log_sums)


def finish_heads(head_out, log_sums, head_gain, heads_local, value_dim):
    tok_rows = head_out.shape[2]
    head_outs = head_out.reshape(heads_local, tok_rows, value_dim)
    normed_heads = (
        head_outs
        * lax.rsqrt(jnp.mean(head_outs * head_outs, axis=2, keepdims=True) + NORM_EPS)
        * head_gain
    )
    attended = jnp.transpose(normed_heads, (1, 0, 2)).reshape(tok_rows, heads_local * value_dim)
    log_out = jnp.transpose(log_sums.reshape(heads_local, 2, tok_rows), (1, 0, 2))
    return (attended, log_out)


def local(
    tokens,
    norm_gain,
    query_weight,
    key_weight,
    value_weight,
    mix_lambda,
    head_gain,
    pool_weight,
    pool_mix,
    pool_scale,
    gate_weight,
    out_weight,
):
    model_width = tokens.shape[1]
    heads_local = query_weight.shape[1]
    kv_local = key_weight.shape[1]
    head_dim = query_weight.shape[2] // 2
    value_dim = value_weight.shape[2]
    groups_local = pool_weight.shape[1]
    group_width = pool_weight.shape[2]
    channels = gate_weight.shape[2]
    matrices = (
        query_weight.reshape(model_width, -1),
        key_weight.reshape(model_width, -1),
        value_weight.reshape(model_width, -1),
        pool_weight.reshape(model_width, -1),
        gate_weight.reshape(model_width, -1),
    )

    def project(rows_piece):
        inputs = rows_piece.astype(jnp.float32)
        normed = (
            inputs
            * lax.rsqrt(jnp.mean(inputs * inputs, axis=1, keepdims=True) + NORM_EPS)
            * norm_gain
        ).astype(jnp.bfloat16)
        return jnp.concatenate(
            [
                jnp.dot(normed, matrix, preferred_element_type=jnp.float32).astype(jnp.bfloat16)
                for matrix in matrices
            ],
            axis=1,
        )

    joined = project(lax.all_gather(tokens, "tp", axis=0, tiled=True))
    tok_rows = joined.shape[0]
    bounds = [0]
    for matrix in matrices:
        bounds.append(bounds[-1] + matrix.shape[1])
    queries = joined[:, bounds[0] : bounds[1]].reshape(
        tok_rows, kv_local, heads_local // kv_local, 2, head_dim
    )
    keys_own = joined[:, bounds[1] : bounds[2]]
    values_own = joined[:, bounds[2] : bounds[3]]
    pool_in = joined[:, bounds[3] : bounds[4]]
    gate_pre = joined[:, bounds[4] : bounds[5]].reshape(tok_rows, 2, channels)
    rim_rows = pool_in[tok_rows - WINDOW :]
    seq_index = lax.axis_index("sp")
    seq_devices = lax.axis_size("sp")
    query_start = seq_index * tok_rows
    near_keys, near_values, rim_prev = shifted((keys_own, values_own, rim_rows), "sp", 1)
    key_buffer = jnp.concatenate([near_keys, keys_own], axis=0)
    value_buffer = jnp.concatenate([near_values, values_own], axis=0)
    reach_devices = 2
    while reach_devices < seq_devices:
        far_keys, far_values = shifted((key_buffer, value_buffer), "sp", reach_devices)
        key_buffer = jnp.concatenate([far_keys, key_buffer], axis=0)
        value_buffer = jnp.concatenate([far_values, value_buffer], axis=0)
        reach_devices = reach_devices * 2
    key_start = query_start - (seq_devices - 1) * tok_rows
    lambda_local = mix_lambda.reshape(kv_local, heads_local // kv_local)
    head_out, log_sums = attend(
        queries, key_buffer, value_buffer, key_start, query_start, lambda_local, head_dim, value_dim
    )
    attended, log_out = finish_heads(head_out, log_sums, head_gain, heads_local, value_dim)
    positions = query_start + jnp.arange(tok_rows, dtype=jnp.int32)
    pool_split = pool_in.reshape(tok_rows, groups_local, group_width)
    extended = (
        jnp.concatenate([rim_prev, pool_in], axis=0)
        .astype(jnp.float32)
        .reshape(WINDOW + tok_rows, groups_local, group_width)
    )
    group_index = lax.axis_index("tp") * groups_local + 0
    window_span = jnp.left_shift(jnp.int32(2), group_index)
    window_sum = jnp.zeros((tok_rows, group_width), jnp.float32)
    for back_rows in range(WINDOW):
        window_sum = window_sum + jnp.where(
            back_rows < window_span,
            extended[WINDOW - back_rows : WINDOW - back_rows + tok_rows, 0],
            0.0,
        )
    counts = jnp.minimum(positions + 1, window_span).astype(jnp.float32)
    means = window_sum / counts[:, None]
    pooled = (means - pool_split[:, 0].astype(jnp.float32)).astype(jnp.bfloat16)
    group_parts = jnp.dot(pooled, pool_mix[0], preferred_element_type=jnp.float32) * pool_scale[0]
    merged = (
        jax.nn.sigmoid(gate_pre[:, 0].astype(jnp.float32)) * attended
        + jax.nn.sigmoid(gate_pre[:, 1].astype(jnp.float32)) * group_parts
    ).astype(jnp.bfloat16)
    mixed = lax.psum_scatter(
        jnp.dot(merged, out_weight, preferred_element_type=jnp.float32).astype(jnp.bfloat16),
        "tp",
        scatter_dimension=0,
        tiled=True,
    )
    return (mixed, log_out)


def solution(mesh):
    in_specs = (
        P(("sp", "tp"), None),
        P(),
        P(None, "tp", None),
        P(None, "tp", None),
        P(None, "tp", None),
        P("tp"),
        P(),
        P(None, "tp", None),
        P("tp", None, None),
        P("tp", None),
        P(None, None, "tp"),
        P("tp", None),
    )
    out_specs = (P(("sp", "tp"), None), P(None, "tp", "sp"))
    return jax.shard_map(local, mesh=mesh, in_specs=in_specs, out_specs=out_specs, check_vma=False)
```

profile of v0, /device:TPU:28, one launch (start us, length us, event | category | flops | bytes accessed | tf_op | source)
XLA Modules:
  0.0 139.2 jit_solution(5411709688306317516)
XLA Ops:
  7.2 0.7 all-gather.2.cloned.1.call-update
  8.0 5.4 %copy.36 = bf16[256,8,2,512]{3,1,2,0:T(8,128)(2,1)} copy(bf16[256,8,2,512]{3,2,1,0:T(2,128)(2,1)} %bitcast.137) | data formatting | bytes 8388608
  13.4 0.6 minimum_convert_fusion
  14.0 13.2 %all-gather.2.cloned.1.call-done = bf16[256,2048]{1,0:T(8,128)(2,1)} async-done(((bf16[64,2048]{1,0:T(8,128)(2,1)}), bf16[256,2048]{1,0:T(8,128)(2,1)}) %all-gather.2.cloned.1.call-update) | async-done | bytes 1048592 | tf_op jit(solution)/shard_map/all_gather | solution.py:134
  27.2 1.6 %fusion.25 = f32[256]{0:T(256)S(1)} fusion(bf16[256,2048]{1,0:T(8,128)(2,1)} %all-gather.2.cloned.1.call-done), kind=kLoop, calls=%fused_computation.32 | loop fusion | flops 1572608 | bytes 1049600 | tf_op jit(solution)/shard_map/reduce_sum | solution.py:123
  28.8 1.9 %convolution_convert_fusion.3 = bf16[256,128]{1,0:T(8,128)(2,1)S(1)} fusion(bf16[2048,1,128]{2,0,1:T(8,128)(2,1)S(1)} %copy-done.12, bf16[256,2048]{1,0:T(8,128)(2,1)} %all-gather.2.cloned.1.call-done, f32[2048]{0:T(1024)S(1)} %copy-done.13, f32[256]{0:T(256)S(1)} %add_rsqrt_fusion.1), kind=kOutput, calls=%fused_computation.48 | convolution fusion | flops 136347648 | bytes 1647616 | tf_op jit(solution)/shard_map/dot_general | solution.py:128
  30.7 1.3 collective-permute-start
  32.0 1.6 %convolution_convert_fusion.2 = bf16[256,128]{1,0:T(8,128)(2,1)S(1)} fusion(bf16[2048,1,128]{2,0,1:T(8,128)(2,1)} %param.18, bf16[256,2048]{1,0:T(8,128)(2,1)S(1)} %copy-done.3, f32[2048]{0:T(1024)S(1)} %copy-done.13, f32[256]{0:T(256)S(1)} %add_rsqrt_fusion.1), kind=kOutput, calls=%fused_computation.47 | convolution fusion | flops 136347648 | bytes 1647616 | tf_op jit(solution)/shard_map/dot_general | solution.py:128
  33.6 1.3 collective-permute-start.3
  34.9 2.1 %convolution_convert_fusion.1 = bf16[256,1024]{1,0:T(8,128)(2,1)} fusion(bf16[2048,1024]{1,0:T(8,128)(2,1)S(1)} %bitcast.138, bf16[256,2048]{1,0:T(8,128)(2,1)S(1)} %copy-done.3, f32[2048]{0:T(1024)S(1)} %copy-done.13, f32[256]{0:T(256)S(1)} %add_rsqrt_fusion.1), kind=kOutput, calls=%fused_computation.40 | convolution fusion | flops 1076101120 | bytes 5776384 | tf_op jit(solution)/shard_map/dot_general | solution.py:128
  37.1 1.3 collective-permute-start.1
  38.4 0.8 fusion.39
  39.2 1.2 collective-permute-done.3
  40.4 1.3 collective-permute-start.4
  41.7 5.4 %collective-permute-done.1 = bf16[512,128]{1,0:T(8,128)(2,1)S(1)} collective-permute-done((bf16[512,128]{1,0:T(8,128)(2,1)S(1)}, bf16[512,128]{1,0:T(8,128)(2,1)S(1)}, u32[]{:S(2)}, u32[]{:S(2)}) %collective-permute-start.1) | collective-permute-done | bytes 131104 | tf_op jit(solution)/shard_map/ppermute | solution.py:17
  47.1 0.7 pad_maximum_fusion.1
  47.8 1.3 collective-permute-start.2
  49.1 0.7 fusion.36
  50.0 2.1 %copy.35 = bf16[256,1024]{0,1:T(8,128)(2,1)} copy(bf16[256,1024]{1,0:T(8,128)(2,1)} %convolution_convert_fusion.1) | data formatting | bytes 1048576 | tf_op jit(solution)/shard_map/reshape | solution.py:145
  52.1 1.3 collective-permute-start.6
  53.4 0.7 pad_maximum_fusion.2
  54.1 1.3 collective-permute-start.5
  55.4 2.3 %collective-permute-done.6 = bf16[16,512]{1,0:T(8,128)(2,1)S(1)} collective-permute-done((bf16[16,512]{1,0:T(8,128)(2,1)S(1)}, bf16[16,512]{1,0:T(8,128)(2,1)S(1)}, u32[]{:S(2)}, u32[]{:S(2)}) %collective-permute-start.6) | collective-permute-done | bytes 16416 | tf_op jit(solution)/shard_map/ppermute | solution.py:17
  57.7 0.9 maximum_convert_fusion
  58.6 11.8 %collective-permute-done.2 = bf16[1024,128]{1,0:T(8,128)(2,1)} collective-permute-done((bf16[1024,128]{1,0:T(8,128)(2,1)}, bf16[1024,128]{1,0:T(8,128)(2,1)}, u32[]{:S(2)}, u32[]{:S(2)}) %collective-permute-start.2) | collective-permute-done | bytes 262176 | tf_op jit(solution)/shard_map/ppermute | solution.py:17
  70.4 1.0 pad_maximum_fusion
  71.3 1.0 copy.25
  72.4 3.0 %collective-permute-done.5 = bf16[1024,128]{1,0:T(8,128)(2,1)} collective-permute-done((bf16[1024,128]{1,0:T(8,128)(2,1)}, bf16[1024,128]{1,0:T(8,128)(2,1)}, u32[]{:S(2)}, u32[]{:S(2)}) %collective-permute-start.5) | collective-permute-done | bytes 262176 | tf_op jit(solution)/shard_map/ppermute | solution.py:17
  75.3 1.8 %maximum_bitcast_fusion = bf16[2048,1,128]{2,0,1:T(8,128)(2,1)} fusion(bf16[256,128]{1,0:T(8,128)(2,1)S(1)} %convolution_convert_fusion.2, bf16[256,128]{1,0:T(8,128)(2,1)S(1)} %collective-permute-done.3, bf16[512,128]{1,0:T(8,128)(2,1)S(1)} %collective-permute-done.4, bf16[1024,128]{1,0:T(8,128)(2,1)} %collective-permute-done.5), kind=kLoop, calls=%fused_computation.89 | loop fusion | flops 2097152 | bytes 1048576 | tf_op jit(solution)/shard_map/reshape | solution.py:27
  77.2 21.6 %while.15 = (s32[]{:T(128)}, f32[1,4,2,256]{3,1,2,0:T(4,128)S(1)}, f32[1,4,2,256]{3,1,2,0:T(4,128)S(1)}, f32[1,4,2,256,128]{4,3,2,1,0:T(8,128)S(1)}, s32[]{:T(12...) while((s32[]{:T(128)}, f32[1,4,2,256]{3,1,2,0:T(4,128)S(1)}, ...), condition=%wide.region_4.5_spmd.clone, body=%wide.region_1.4_spmd.clone.sunk | while | flops 411836160 | bytes 15744211 | solution.py:66
  77.5 1.7 %fusion.134 = (f32[4,2,256]{2,0,1:T(4,128)S(1)}, f32[2,512,256,4]{2,1,3,0:T(8,128)S(1)}) fusion(pred[256,512]{0,1:T(8,128)(4,1)S(1)} %compare_and_fusion.2, bf16[256,1,4,2,64]{0,4,2,3,1:T(8,128)(2,1)S(1)} %get-tuple-element.243, bf16[2048,1,2,64]{0,3,2,1:T(8,128)(2,1)} %get-tuple-element.242, s32[]{:T(128)S(6)} %select_n.393), kind=kOutput, calls=%fused_computation.3.clone.1 | convolution fusion | flops 137361408 | bytes 4726788 | tf_op jit(solution)/shard_map/while/body/qgrmd,kgmd->grmqk/dot_general | solution.py:40
  79.2 1.0 fusion.136
  80.3 2.3 %fusion.137 = f32[1,4,2,256,128]{4,3,2,1,0:T(8,128)S(1)} fusion(bf16[4,2,256,512]{2,3,0,1:T(8,128)(2,1)S(1)} %get-tuple-element.206, f32[1,4,2,256,128]{4,3,2,1,0:T(8,128)S(1)} %get-tuple-element.225, f32[4,2,256]{2,1,0:T(2,128)S(1)} %copy.53, bf16[2048,1,128]{2,0,1:T(8,128)(2,1)} %get-tuple-element.244, s32[]{:T(128)S(6)} %select_n.393), kind=kOutput, calls=%fused_computation.12.clone.1 | convolution fusion | flops 268959744 | bytes 4333572 | tf_op jit(solution)/shard_map/while/body/grmqk,kgd->grmqd/dot_general | solution.py:53
  82.9 1.7 %fusion.134 = (f32[4,2,256]{2,0,1:T(4,128)S(1)}, f32[2,512,256,4]{2,1,3,0:T(8,128)S(1)}) fusion(pred[256,512]{0,1:T(8,128)(4,1)S(1)} %compare_and_fusion.2, bf16[256,1,4,2,64]{0,4,2,3,1:T(8,128)(2,1)S(1)} %get-tuple-element.243, bf16[2048,1,2,64]{0,3,2,1:T(8,128)(2,1)} %get-tuple-element.242, s32[]{:T(128)S(6)} %select_n.393), kind=kOutput, calls=%fused_computation.3.clone.1 | convolution fusion | flops 137361408 | bytes 4726788 | tf_op jit(solution)/shard_map/while/body/qgrmd,kgmd->grmqk/dot_general | solution.py:40
  84.6 1.0 fusion.136
  85.6 2.3 %fusion.137 = f32[1,4,2,256,128]{4,3,2,1,0:T(8,128)S(1)} fusion(bf16[4,2,256,512]{2,3,0,1:T(8,128)(2,1)S(1)} %get-tuple-element.206, f32[1,4,2,256,128]{4,3,2,1,0:T(8,128)S(1)} %get-tuple-element.225, f32[4,2,256]{2,1,0:T(2,128)S(1)} %copy.53, bf16[2048,1,128]{2,0,1:T(8,128)(2,1)} %get-tuple-element.244, s32[]{:T(128)S(6)} %select_n.393), kind=kOutput, calls=%fused_computation.12.clone.1 | convolution fusion | flops 268959744 | bytes 4333572 | tf_op jit(solution)/shard_map/while/body/grmqk,kgd->grmqd/dot_general | solution.py:53
  88.2 1.7 %fusion.134 = (f32[4,2,256]{2,0,1:T(4,128)S(1)}, f32[2,512,256,4]{2,1,3,0:T(8,128)S(1)}) fusion(pred[256,512]{0,1:T(8,128)(4,1)S(1)} %compare_and_fusion.2, bf16[256,1,4,2,64]{0,4,2,3,1:T(8,128)(2,1)S(1)} %get-tuple-element.243, bf16[2048,1,2,64]{0,3,2,1:T(8,128)(2,1)} %get-tuple-element.242, s32[]{:T(128)S(6)} %select_n.393), kind=kOutput, calls=%fused_computation.3.clone.1 | convolution fusion | flops 137361408 | bytes 4726788 | tf_op jit(solution)/shard_map/while/body/qgrmd,kgmd->grmqk/dot_general | solution.py:40
  90.0 1.0 fusion.136
  91.0 2.3 %fusion.137 = f32[1,4,2,256,128]{4,3,2,1,0:T(8,128)S(1)} fusion(bf16[4,2,256,512]{2,3,0,1:T(8,128)(2,1)S(1)} %get-tuple-element.206, f32[1,4,2,256,128]{4,3,2,1,0:T(8,128)S(1)} %get-tuple-element.225, f32[4,2,256]{2,1,0:T(2,128)S(1)} %copy.53, bf16[2048,1,128]{2,0,1:T(8,128)(2,1)} %get-tuple-element.244, s32[]{:T(128)S(6)} %select_n.393), kind=kOutput, calls=%fused_computation.12.clone.1 | convolution fusion | flops 268959744 | bytes 4333572 | tf_op jit(solution)/shard_map/while/body/grmqk,kgd->grmqd/dot_general | solution.py:53
  93.6 1.7 %fusion.134 = (f32[4,2,256]{2,0,1:T(4,128)S(1)}, f32[2,512,256,4]{2,1,3,0:T(8,128)S(1)}) fusion(pred[256,512]{0,1:T(8,128)(4,1)S(1)} %compare_and_fusion.2, bf16[256,1,4,2,64]{0,4,2,3,1:T(8,128)(2,1)S(1)} %get-tuple-element.243, bf16[2048,1,2,64]{0,3,2,1:T(8,128)(2,1)} %get-tuple-element.242, s32[]{:T(128)S(6)} %select_n.393), kind=kOutput, calls=%fused_computation.3.clone.1 | convolution fusion | flops 137361408 | bytes 4726788 | tf_op jit(solution)/shard_map/while/body/qgrmd,kgmd->grmqk/dot_general | solution.py:40
  95.3 1.0 fusion.136
  96.3 2.3 %fusion.137 = f32[1,4,2,256,128]{4,3,2,1,0:T(8,128)S(1)} fusion(bf16[4,2,256,512]{2,3,0,1:T(8,128)(2,1)S(1)} %get-tuple-element.206, f32[1,4,2,256,128]{4,3,2,1,0:T(8,128)S(1)} %get-tuple-element.225, f32[4,2,256]{2,1,0:T(2,128)S(1)} %copy.53, bf16[2048,1,128]{2,0,1:T(8,128)(2,1)} %get-tuple-element.244, s32[]{:T(128)S(6)} %select_n.393), kind=kOutput, calls=%fused_computation.12.clone.1 | convolution fusion | flops 268959744 | bytes 4333572 | tf_op jit(solution)/shard_map/while/body/grmqk,kgd->grmqd/dot_general | solution.py:53
  98.9 1.3 copy.28
  100.3 1.5 %multiply_reduce_fusion = (f32[4,256]{1,0:T(4,128)S(1)}, f32[4,256,128]{1,2,0:T(8,128)S(1)}) fusion(f32[4,256]{1,0:T(4,128)S(1)} %get-tuple-element.133, f32[1,4,2,256,128]{3,4,1,2,0:T(8,128)} %copy.28, f32[4]{0:T(128)S(1)} %copy-done.8, f32[4,256]{1,0:T(4,128)S(1)} %get-tuple-element.132), kind=kLoop, calls=%fused_computation.101 | loop fusion | flops 785408 | bytes 1585168 | tf_op jit(solution)/shard_map/reduce_sum | solution.py:81
  101.9 1.0 bitcast_multiply_fusion
  102.9 4.5 %convolution_convert_fusion = bf16[256,2048]{1,0:T(8,128)(2,1)} fusion(bf16[512,2048]{1,0:T(8,128)(2,1)S(1)} %copy-done, f32[256,512]{0,1:T(8,128)} %bitcast_multiply_fusion, bf16[1,512,512]{2,1,0:T(8,128)(2,1)} %param.22, bf16[256,512]{1,0:T(8,128)(2,1)S(1)} %copy-done.6, f32[272,512]{1,0:T(8,128)S(1)} %copy-done.4, ...), kind=kOutput, calls=%fused_computation.31 | convolution fusion | flops 677249024 | bytes 13110288 | tf_op jit(solution)/shard_map/dot_general | solution.py:190
  107.4 0.6 add_bitcast_fusion
  108.0 24.4 %reduce-scatter.2.cloned.1.call-done = bf16[64,2048]{1,0:T(8,128)(2,1)} async-done(((bf16[256,2048]{1,0:T(8,128)(2,1)}), bf16[64,2048]{1,0:T(8,128)(2,1)}) %reduce-scatter.2.cloned.1.call-update) | async-done | bytes 262160 | tf_op jit(solution)/shard_map/reduce_scatter | solution.py:189
  (79 shorter events, 1.6 us)
Async XLA Ops:
  7.2 95.7 %copy-start = (bf16[512,2048]{1,0:T(8,128)(2,1)S(1)}, bf16[512,2048]{1,0:T(8,128)(2,1)}, u32[]{:S(2)}) copy-start(bf16[512,2048]{1,0:T(8,128)(2,1)} %param.25) | copy-start | bytes 6291460
  7.2 20.0 %all-gather.2.cloned.1.call-start = ((), (), s32[]{:S(2)}) async-start(), calls=%async_computation.1 | async-start | bytes 1310720 | tf_op jit(solution)/shard_map/all_gather | solution.py:134
  7.9 124.4 %reduce-scatter.2.cloned.1.call-start = ((), (), s32[]{:S(2)}) async-start(), calls=%async_computation.2 | async-start | bytes 1310720 | tf_op jit(solution)/shard_map/reduce_scatter | solution.py:189
  8.0 20.8 %copy-start.12 = (bf16[2048,1,128]{2,0,1:T(8,128)(2,1)S(1)}, bf16[2048,1,128]{2,0,1:T(8,128)(2,1)}, u32[]{:S(2)}) copy-start(bf16[2048,1,128]{2,0,1:T(8,128)(2,1)} %param.17) | copy-start | bytes 1572868
  8.0 20.8 %copy-start.13 = (f32[2048]{0:T(1024)S(1)}, f32[2048]{0:T(1024)}, u32[]{:S(2)}) copy-start(f32[2048]{0:T(1024)} %param.15) | copy-start | bytes 24580
  27.2 4.8 %copy-start.3 = (bf16[256,2048]{1,0:T(8,128)(2,1)S(1)}, bf16[256,2048]{1,0:T(8,128)(2,1)}, u32[]{:S(2)}) copy-start(bf16[256,2048]{1,0:T(8,128)(2,1)} %all-gather.2.cloned.1.call-done) | copy-start | bytes 3145732
  28.8 6.1 %copy-start.1 = (bf16[256,8,2,512]{3,1,2,0:T(8,128)(2,1)S(1)}, bf16[256,8,2,512]{3,1,2,0:T(8,128)(2,1)}, u32[]{:S(2)}) copy-start(bf16[256,8,2,512]{3,1,2,0:T(8,128)(2,1)} %copy.36) | copy-start | bytes 12582916
  30.7 6.3 %collective-permute-start = (bf16[256,128]{1,0:T(8,128)(2,1)S(1)}, bf16[256,128]{1,0:T(8,128)(2,1)S(1)}, u32[]{:S(2)}, u32[]{:S(2)}) collective-permute-start(bf16[256,128]{1,0:T(8,128)(2,1)S(1)} %convolution_convert_fusion.3), channel_id=1, source_target_pairs={{0,4},{4,8},{8,12},{12,16},{16,20},{20,24},{24,28},{1,5},{5,9},{9,... | collective-permute-start | bytes 196616 | tf_op jit(solution)/shard_map/ppermute | solution.py:17
  33.6 6.8 %collective-permute-start.3 = (bf16[256,128]{1,0:T(8,128)(2,1)S(1)}, bf16[256,128]{1,0:T(8,128)(2,1)S(1)}, u32[]{:S(2)}, u32[]{:S(2)}) collective-permute-start(bf16[256,128]{1,0:T(8,128)(2,1)S(1)} %convolution_convert_fusion.2), channel_id=1, source_target_pairs={{0,4},{4,8},{8,12},{12,16},{16,20},{20,24},{24,28},{1,5},{5,9},{9,... | collective-permute-start | bytes 196616 | tf_op jit(solution)/shard_map/ppermute | solution.py:17
  34.9 3.5 %copy-start.10 = (bf16[2048,4,128]{2,1,0:T(4,128)(2,1)S(1)}, bf16[2048,4,128]{2,1,0:T(4,128)(2,1)}, u32[]{:S(2)}) copy-start(bf16[2048,4,128]{2,1,0:T(4,128)(2,1)} %param.16) | copy-start | bytes 6291460
  37.1 10.0 %collective-permute-start.1 = (bf16[512,128]{1,0:T(8,128)(2,1)S(1)}, bf16[512,128]{1,0:T(8,128)(2,1)S(1)}, u32[]{:S(2)}, u32[]{:S(2)}) collective-permute-start(bf16[512,128]{1,0:T(8,128)(2,1)S(1)} %pad_maximum_fusion.3), channel_id=1, source_target_pairs={{0,8},{4,12},{8,16},{12,20},{16,24},{20,28},{1,9},{5,13},{9,17},{1... | collective-permute-start | bytes 393224 | tf_op jit(solution)/shard_map/ppermute | solution.py:17
  38.4 10.7 %copy-start.11 = (bf16[2048,1,512]{2,0,1:T(8,128)(2,1)S(1)}, bf16[2048,1,512]{2,0,1:T(8,128)(2,1)}, u32[]{:S(2)}) copy-start(bf16[2048,1,512]{2,0,1:T(8,128)(2,1)} %param.21) | copy-start | bytes 6291460
  40.4 13.0 %collective-permute-start.4 = (bf16[512,128]{1,0:T(8,128)(2,1)S(1)}, bf16[512,128]{1,0:T(8,128)(2,1)S(1)}, u32[]{:S(2)}, u32[]{:S(2)}) collective-permute-start(bf16[512,128]{1,0:T(8,128)(2,1)S(1)} %pad_maximum_fusion.4), channel_id=1, source_target_pairs={{0,8},{4,12},{8,16},{12,20},{16,24},{20,28},{1,9},{5,13},{9,17},{1... | collective-permute-start | bytes 393224 | tf_op jit(solution)/shard_map/ppermute | solution.py:17
  47.8 22.6 %collective-permute-start.2 = (bf16[1024,128]{1,0:T(8,128)(2,1)}, bf16[1024,128]{1,0:T(8,128)(2,1)}, u32[]{:S(2)}, u32[]{:S(2)}) collective-permute-start(bf16[1024,128]{1,0:T(8,128)(2,1)} %pad_maximum_fusion.1), channel_id=1, source_target_pairs={{0,16},{4,20},{8,24},{12,28},{1,17},{5,21},{9,25},{13,29},{2,18},{... | collective-permute-start | bytes 786440 | tf_op jit(solution)/shard_map/ppermute | solution.py:17
  49.8 8.8 %copy-start.5 = (bf16[256,512]{1,0:T(8,128)(2,1)}, bf16[256,512]{1,0:T(8,128)(2,1)S(1)}, u32[]{:S(2)}) copy-start(bf16[256,512]{1,0:T(8,128)(2,1)S(1)} %fusion.36) | copy-start | bytes 786436
  52.1 5.6 %collective-permute-start.6 = (bf16[16,512]{1,0:T(8,128)(2,1)S(1)}, bf16[16,512]{1,0:T(8,128)(2,1)S(1)}, u32[]{:S(2)}, u32[]{:S(2)}) collective-permute-start(bf16[16,512]{1,0:T(8,128)(2,1)S(1)} %slice.112), channel_id=1, source_target_pairs={{0,4},{4,8},{8,12},{12,16},{16,20},{20,24},{24,28},{1,5},{5,9},{9,... | collective-permute-start | bytes 49160 | tf_op jit(solution)/shard_map/ppermute | solution.py:17
  54.1 21.2 %collective-permute-start.5 = (bf16[1024,128]{1,0:T(8,128)(2,1)}, bf16[1024,128]{1,0:T(8,128)(2,1)}, u32[]{:S(2)}, u32[]{:S(2)}) collective-permute-start(bf16[1024,128]{1,0:T(8,128)(2,1)} %pad_maximum_fusion.2), channel_id=1, source_target_pairs={{0,16},{4,20},{8,24},{12,28},{1,17},{5,21},{9,25},{13,29},{2,18},{... | collective-permute-start | bytes 786440 | tf_op jit(solution)/shard_map/ppermute | solution.py:17
  98.9 1.4 copy-start.8
  98.9 2.8 %copy-start.9 = (f32[128]{0:T(128)S(1)}, f32[128]{0:T(128)}, u32[]{:S(2)}) copy-start(f32[128]{0:T(128)} %param.20) | copy-start | bytes 1540
  100.2 1.6 %copy-start.2 = (bf16[256,1024]{0,1:T(8,128)(2,1)S(1)}, bf16[256,1024]{0,1:T(8,128)(2,1)}, u32[]{:S(2)}) copy-start(bf16[256,1024]{0,1:T(8,128)(2,1)} %copy.35) | copy-start | bytes 1572868
  100.2 2.6 %copy-start.4 = (f32[272,512]{1,0:T(8,128)S(1)}, f32[272,512]{1,0:T(8,128)}, u32[]{:S(2)}) copy-start(f32[272,512]{1,0:T(8,128)} %maximum_convert_fusion) | copy-start | bytes 1671172
  100.2 2.6 %copy-start.6 = (bf16[256,512]{1,0:T(8,128)(2,1)S(1)}, bf16[256,512]{1,0:T(8,128)(2,1)}, u32[]{:S(2)}) copy-start(bf16[256,512]{1,0:T(8,128)(2,1)} %copy-done.5) | copy-start | bytes 786436
  100.2 2.6 %copy-start.7 = (f32[256]{0:T(256)S(1)}, f32[256]{0:T(256)}, u32[]{:S(2)}) copy-start(f32[256]{0:T(256)} %minimum_convert_fusion) | copy-start | bytes 3076
  100.2 2.6 %copy-start.14 = (f32[1,512]{1,0:T(1,128)S(1)}, f32[1,512]{1,0:T(1,128)}, u32[]{:S(2)}) copy-start(f32[1,512]{1,0:T(1,128)} %param.23) | copy-start | bytes 6148
Sparse Core Ops, SparseCore 0:
  9.5 17.6 all-gather.1
  107.5 24.8 reduce-scatter.1
where the time goes:
time: 142 us; the launch traced here: 139 us
  waiting for transfers between devices  61.9 us (44%)
  matrix products  27.6 us (19%)
  other arithmetic  15.4 us (11%)
  between operations  14.4 us (10%)
  local copies, waits for them, and re-layouts  10.1 us (7%)
  starting transfers between devices  9.08 us (6%)
    reduce_scatter x1, waiting for transfers between devices, local(): lax.psum_scatter(jnp.dot(merged, out_weight, preferred_element_type=jnp.f...  24.4 us
    ppermute x7, waiting for transfers between devices, shifted(): return lax.ppermute(block, axis, route)  23.6 us
    all_gather x1, waiting for transfers between devices, local(): joined = project(lax.all_gather(tokens, 'tp', axis=0, tiled=True))  13.2 us
    dot_general x4, matrix products, online_step(): jnp.einsum('grmqk,kgd->grmqd', probs.astype(jnp.bfloat16), block_values,...  9.18 us
    ppermute x7, starting transfers between devices, shifted(): return lax.ppermute(block, axis, route)  9.01 us
    dot_general x5, matrix products, project(): jnp.dot(normed, matrix, preferred_element_type=jnp.float32)  7.07 us
    dot_general x4, matrix products, online_step(): jnp.einsum('qgrmd,kgmd->grmqk', queries, block_keys_arr, preferred_elemen...  6.9 us
    unnamed x32, local copies, waits for them, and re-layouts  5.48 us
  transfers between devices with their start and end apart: 9, of which 7 were waited for; matrix products, arithmetic and copies ran while one was open for 13% of the time, Pallas kernels for 0%

commit v1 on v0

v1 whole, which is shorter than its diff:
```python
import functools

import jax
import jax.numpy as jnp
from jax import lax
from jax.experimental import pallas as pl
from jax.experimental.pallas import tpu as pltpu
from jax.sharding import PartitionSpec as P

WINDOW = 16
NORM_EPS = 1e-06
MESH = pl.DeviceIdType.MESH
F32 = jnp.float32
BF16 = jnp.bfloat16
COLS = 256


def layer_kernel(
    S, T, heads, dims,
    lam_ref, tokens, gain_ref, wq_h, wk_h, wv_h, hgain_ref, wp_h, mix_h, pscale_ref, wg_h, wo_h,
    out_ref, lse_ref,
    tok, nrm, wkv, wq, wp, wg, wmix, wo, kvb, qt, acc, m_ref, l_ref, pool, gates, rim_out, rim_in,
    merged, part_remote, part_near, got_pair, got_near, sum_out, got_sum, keep,
    load_sem, tsend, trecv, ksend, krecv, rsem, psend, precv, ssend, srecv,
):
    R, HD, DV, GW, D = dims
    A = T // 2
    HALF = 2 * R
    rows = T * R
    QC = 2 * rows
    s = lax.axis_index("sp")
    t = lax.axis_index("tp")
    a = t // 2
    b = t % 2
    z = s // 2
    y = s % 2
    mate_t = 2 * a + 1 - b
    mate_s = 2 * z + 1 - y

    def slot(i):
        return pl.ds(pl.multiple_of(i * R, R), R)

    loads = [
        pltpu.make_async_copy(tokens, tok.at[slot(t)], load_sem.at[0]),
        pltpu.make_async_copy(wk_h, wkv.at[:, pl.ds(0, 2 * HD)], load_sem.at[1]),
        pltpu.make_async_copy(wv_h, wkv.at[:, pl.ds(2 * HD, DV)], load_sem.at[2]),
        pltpu.make_async_copy(wq_h, wq, load_sem.at[3]),
        pltpu.make_async_copy(wp_h, wp, load_sem.at[4]),
        pltpu.make_async_copy(wg_h, wg, load_sem.at[5]),
        pltpu.make_async_copy(mix_h, wmix, load_sem.at[6]),
        pltpu.make_async_copy(wo_h, wo, load_sem.at[7]),
    ]
    for load in loads:
        load.start()

    barrier = pltpu.get_barrier_semaphore()
    count = T - 1
    for d in range(1, T):
        pl.semaphore_signal(barrier, inc=1, device_id={"tp": (t + d) % T}, device_id_type=MESH)
    for d in (1, -1, 2, -2):
        ok = jnp.logical_and(s + d >= 0, s + d < S)

        @pl.when(ok)
        def _():
            pl.semaphore_signal(barrier, inc=1, device_id={"sp": s + d}, device_id_type=MESH)

        count = count + ok.astype(jnp.int32)
    pl.semaphore_wait(barrier, count)

    def tok_copy(i, lane, dst):
        return pltpu.make_async_remote_copy(
            src_ref=tok.at[slot(i)], dst_ref=tok.at[slot(i)],
            send_sem=tsend.at[lane], recv_sem=trecv.at[i],
            device_id={"tp": dst}, device_id_type=MESH)

    loads[0].wait()
    tok_sends = []
    for i in range(1, A):
        c = tok_copy(t, i, 2 * ((a + i) % A) + b)
        c.start()
        tok_sends.append(c)
    c = tok_copy(t, 0, mate_t)
    c.start()
    tok_sends.append(c)

    def kv_copy(j, p, lane, dst):
        return pltpu.make_async_remote_copy(
            src_ref=kvb.at[j, p], dst_ref=kvb.at[j, p],
            send_sem=ksend.at[(j * A + p) * 2 + lane], recv_sem=krecv.at[j * A + p],
            device_id={"sp": dst}, device_id_type=MESH)

    has_next = s + 2 < S

    def project_half(p):
        at = pl.ds(pl.multiple_of(p * HALF, HALF), HALF)
        x = tok[at].astype(F32)
        n = (x * lax.rsqrt(jnp.mean(x * x, axis=1, keepdims=True) + NORM_EPS) * gain_ref[...]).astype(BF16)
        nrm[at] = n
        kvb[s, p] = jnp.dot(n, wkv[...], preferred_element_type=F32).astype(BF16)

    def send_half(p):
        @pl.when(has_next)
        def _():
            kv_copy(s, p, 0, s + 2).start()

        @pl.when(y == 0)
        def _():
            kv_copy(s, p, 1, mate_s).start()

    tok_copy(mate_t, 0, mate_t).wait_recv()
    loads[1].wait()
    loads[2].wait()
    project_half(a)
    send_half(a)
    for i in range(1, A):
        far = (a + i) % A
        tok_copy(2 * far + b, 0, mate_t).wait_recv()
        c = tok_copy(2 * far + b, A - 1 + i, mate_t)
        c.start()
        tok_sends.append(c)
    for i in range(1, A):
        far = (a + i) % A
        tok_copy(2 * far + 1 - b, 0, mate_t).wait_recv()
        project_half(far)
        send_half(far)

    loads[3].wait()
    lane = lax.broadcasted_iota(jnp.int32, (rows, 2 * HD), 1)
    qscale = HD ** -0.5
    for h in range(heads):
        q = jnp.dot(nrm[...], wq[:, h * 2 * HD:(h + 1) * 2 * HD], preferred_element_type=F32)
        q = q.astype(BF16).astype(F32) * qscale
        qt[:, h * QC:h * QC + rows] = jnp.where(lane < HD, q, 0.0).T.astype(BF16)
        qt[:, h * QC + rows:(h + 1) * QC] = jnp.where(lane >= HD, q, 0.0).T.astype(BF16)

    loads[4].wait()
    for c0 in range(0, GW, COLS):
        pool[:, c0:c0 + COLS] = jnp.dot(nrm[...], wp[:, c0:c0 + COLS], preferred_element_type=F32).astype(BF16)
    rim_out[...] = pool[rows - WINDOW:, :]

    def rim_copy(dst):
        return pltpu.make_async_remote_copy(
            src_ref=rim_out, dst_ref=rim_in, send_sem=rsem.at[0], recv_sem=rsem.at[1],
            device_id={"sp": dst}, device_id_type=MESH)

    m_ref[...] = jnp.full_like(m_ref, -1e30)
    l_ref[...] = jnp.zeros_like(l_ref)
    acc[...] = jnp.zeros_like(acc)

    def attend(j, masked):
        blk = kvb[j].reshape(rows, 2 * HD + DV)
        keys = blk[:, :2 * HD]
        vt = blk[:, 2 * HD:].astype(F32).T.astype(BF16)
        if masked:
            ki = lax.broadcasted_iota(jnp.int32, (rows, QC), 0)
            qi = lax.broadcasted_iota(jnp.int32, (rows, QC), 1)
            qi = jnp.where(qi >= rows, qi - rows, qi)
            seen = ki <= qi
        for h in range(heads):
            cs = slice(h * QC, (h + 1) * QC)
            sc = jnp.dot(keys, qt[:, cs], preferred_element_type=F32)
            if masked:
                sc = jnp.where(seen, sc, -1e30)
            m_old = m_ref[:, cs]
            m_new = jnp.maximum(m_old, jnp.max(sc, axis=0, keepdims=True))
            p = jnp.exp(sc - m_new)
            if masked:
                p = jnp.where(seen, p, 0.0)
            alpha = jnp.exp(m_old - m_new)
            l_ref[:, cs] = l_ref[:, cs] * alpha + jnp.sum(p, axis=0, keepdims=True)
            acc[:, cs] = acc[:, cs] * alpha + jnp.dot(vt, p.astype(BF16), preferred_element_type=F32)
            m_ref[:, cs] = m_new

    @pl.when(s + 1 < S)
    def _():
        rim_copy(s + 1).start()

    attend(s, True)

    def chain(k, carry):
        j = 2 * (z - k) + y
        for p in range(A):
            kv_copy(j, p, 0, mate_s).wait_recv()

            @pl.when(has_next)
            def _():
                kv_copy(j, p, 0, s + 2).start()

            kv_copy(j, p, 1, mate_s).start()
        attend(j, False)
        return carry

    lax.fori_loop(1, z + 1, chain, 0)

    loads[5].wait()
    for c0 in range(0, 2 * GW, COLS):
        gates[:, c0:c0 + COLS] = jnp.dot(nrm[...], wg[:, c0:c0 + COLS], preferred_element_type=F32).astype(BF16)

    def mates(k, carry):
        j = 2 * (z - k) + 1 - y
        for p in range(A):
            kv_copy(j, p, 0, mate_s).wait_recv()
        attend(j, False)
        return carry

    @pl.when(s > 0)
    def _():
        rim_copy(s).wait_recv()

    @pl.when(s == 0)
    def _():
        rim_in[...] = jnp.zeros_like(rim_in)

    span = jnp.left_shift(jnp.int32(2), t)
    ri = lax.broadcasted_iota(jnp.int32, (rows, rows), 0)
    ci = lax.broadcasted_iota(jnp.int32, (rows, rows), 1)
    band = jnp.where(jnp.logical_and(ci <= ri, ci > ri - span), 1.0, 0.0).astype(BF16)
    ri2 = lax.broadcasted_iota(jnp.int32, (rows, WINDOW), 0)
    ci2 = lax.broadcasted_iota(jnp.int32, (rows, WINDOW), 1) - WINDOW
    band2 = jnp.where(ci2 > ri2 - span, 1.0, 0.0).astype(BF16)
    pos = s * rows + lax.broadcasted_iota(jnp.int32, (rows, 1), 0)
    counts = jnp.minimum(pos + 1, span).astype(F32)
    total = jnp.dot(band, pool[...], preferred_element_type=F32) + jnp.dot(
        band2, rim_in[...], preferred_element_type=F32)
    pooled = (total / counts - pool[...].astype(F32)).astype(BF16)
    loads[6].wait()
    pmixed = jnp.dot(pooled, wmix[...], preferred_element_type=F32) * pscale_ref[...]
    keep_pool = jax.nn.sigmoid(gates[:, GW:].astype(F32)) * pmixed
    keep[...] = keep_pool

    lax.fori_loop(1 - y, z + 1, mates, 0)

    for h in range(heads):
        c1 = slice(h * QC, h * QC + rows)
        c2 = slice(h * QC + rows, (h + 1) * QC)
        l1 = l_ref[:, c1]
        l2 = l_ref[:, c2]
        lse_ref[0, h:h + 1, :] = m_ref[:, c1] + jnp.log(l1)
        lse_ref[1, h:h + 1, :] = m_ref[:, c2] + jnp.log(l2)
        o = acc[:, c1] / l1 - lam_ref[h] * (acc[:, c2] / l2)
        o = o * lax.rsqrt(jnp.mean(o * o, axis=0, keepdims=True) + NORM_EPS)
        att = o.T * hgain_ref[...]
        hs = slice(h * DV, (h + 1) * DV)
        merged[:, hs] = (jax.nn.sigmoid(gates[:, hs].astype(F32)) * att + keep[:, hs]).astype(BF16)

    loads[7].wait()

    def product(i):
        return jnp.dot(merged[slot(i)], wo[...], preferred_element_type=F32)

    def pair_copy(i):
        return pltpu.make_async_remote_copy(
            src_ref=part_remote.at[i - 1], dst_ref=got_pair.at[i - 1],
            send_sem=psend.at[i], recv_sem=precv.at[i],
            device_id={"tp": mate_t}, device_id_type=MESH)

    near_copy = pltpu.make_async_remote_copy(
        src_ref=part_near, dst_ref=got_near, send_sem=psend.at[0], recv_sem=precv.at[0],
        device_id={"tp": mate_t}, device_id_type=MESH)

    def sum_copy(i):
        return pltpu.make_async_remote_copy(
            src_ref=sum_out.at[i - 1], dst_ref=got_sum.at[i - 1],
            send_sem=ssend.at[i], recv_sem=srecv.at[i],
            device_id={"tp": 2 * ((a + i) % A) + b}, device_id_type=MESH)

    for i in range(1, A):
        far = (a + i) % A
        part_remote[i - 1] = product(2 * far + 1 - b).astype(BF16)
        pair_copy(i).start()
    for i in range(1, A):
        far = (a + i) % A
        mine = product(2 * far + b)
        pair_copy(i).wait_recv()
        sum_out[i - 1] = (mine + got_pair[i - 1].astype(F32)).astype(BF16)
        sum_copy(i).start()
    part_near[...] = product(mate_t).astype(BF16)
    near_copy.start()
    result = product(t)
    near_copy.wait_recv()
    result = result + got_near[...].astype(F32)
    for i in range(1, A):
        sum_copy(i).wait_recv()
        result = result + got_sum[i - 1].astype(F32)
    out_ref[...] = result.astype(BF16)

    for c in tok_sends:
        c.wait_send()

    @pl.when(s + 1 < S)
    def _():
        rim_copy(s + 1).wait_send()

    def drain(k, carry):
        j = 2 * (z - k) + y
        for p in range(A):
            @pl.when(has_next)
            def _():
                kv_copy(j, p, 0, s + 2).wait_send()

            @pl.when(jnp.logical_or(k > 0, y == 0))
            def _():
                kv_copy(j, p, 1, mate_s).wait_send()
        return carry

    lax.fori_loop(0, z + 1, drain, 0)
    near_copy.wait_send()
    for i in range(1, A):
        pair_copy(i).wait_send()
        sum_copy(i).wait_send()


def local(
    tokens, norm_gain, query_weight, key_weight, value_weight, mix_lambda, head_gain,
    pool_weight, pool_mix, pool_scale, gate_weight, out_weight,
):
    S = lax.axis_size("sp")
    T = lax.axis_size("tp")
    A = T // 2
    R, D = tokens.shape
    heads = query_weight.shape[1]
    HD = query_weight.shape[2] // 2
    DV = value_weight.shape[2]
    GW = pool_weight.shape[2]
    rows = T * R
    kv_width = 2 * HD + DV
    columns = heads * 2 * rows
    assert key_weight.shape[1] == 1 and pool_weight.shape[1] == 1
    assert T % 2 == 0 and S % 2 == 0
    hbm = pl.BlockSpec(memory_space=pl.ANY)
    vmem = pl.BlockSpec(memory_space=pltpu.VMEM)
    smem = pl.BlockSpec(memory_space=pltpu.SMEM)
    dma = pltpu.SemaphoreType.DMA
    V = pltpu.VMEM
    return pl.pallas_call(
        functools.partial(layer_kernel, S, T, heads, (R, HD, DV, GW, D)),
        out_shape=(
            jax.ShapeDtypeStruct((R, D), BF16),
            jax.ShapeDtypeStruct((2, heads, rows), F32),
        ),
        in_specs=[smem, hbm, vmem, hbm, hbm, hbm, vmem, hbm, hbm, vmem, hbm, hbm],
        out_specs=(vmem, vmem),
        scratch_shapes=[
            V((rows, D), BF16), V((rows, D), BF16), V((D, kv_width), BF16),
            V((D, heads * 2 * HD), BF16), V((D, GW), BF16), V((D, 2 * GW), BF16),
            V((GW, GW), BF16), V((heads * DV, D), BF16),
            V((S, A, 2 * R, kv_width), BF16), V((2 * HD, columns), BF16), V((DV, columns), F32),
            V((1, columns), F32), V((1, columns), F32), V((rows, GW), BF16), V((rows, 2 * GW), BF16),
            V((WINDOW, GW), BF16), V((WINDOW, GW), BF16), V((rows, GW), BF16),
            V((A - 1, R, D), BF16), V((R, D), BF16), V((A - 1, R, D), BF16), V((R, D), BF16),
            V((A - 1, R, D), BF16), V((A - 1, R, D), BF16), V((rows, GW), F32),
            dma((8,)), dma((2 * A,)), dma((T,)), dma((S * A * 2,)), dma((S * A,)), dma((2,)),
            dma((A,)), dma((A,)), dma((A,)), dma((A,)),
        ],
        compiler_params=pltpu.CompilerParams(
            collective_id=0, has_side_effects=True, vmem_limit_bytes=60 * 1024 * 1024),
    )(
        mix_lambda, tokens, norm_gain.reshape(1, D), query_weight.reshape(D, -1),
        key_weight.reshape(D, -1), value_weight.reshape(D, -1), head_gain.reshape(1, DV),
        pool_weight.reshape(D, -1), pool_mix.reshape(GW, GW), pool_scale,
        gate_weight.reshape(D, -1), out_weight,
    )


def solution(mesh):
    in_specs = (
        P(("sp", "tp"), None), P(), P(None, "tp", None), P(None, "tp", None), P(None, "tp", None),
        P("tp"), P(), P(None, "tp", None), P("tp", None, None), P("tp", None),
        P(None, None, "tp"), P("tp", None),
    )
    out_specs = (P(("sp", "tp"), None), P(None, "tp", "sp"))
    return jax.shard_map(local, mesh=mesh, in_specs=in_specs, out_specs=out_specs, check_vma=False)
```

time: 142 us -> 53.6 us (0.38); the launches traced: 139 us -> 53.4 us
  waiting for transfers between devices: 61.9 us -> 0 us
  Pallas kernels: 0 us -> 43.2 us
  matrix products: 27.6 us -> 0 us
  other arithmetic: 15.4 us -> 0 us
  between operations: 14.4 us -> 0.65 us
  starting transfers between devices: 9.08 us -> 0 us
    pallas_call x0 -> x1, Pallas kernels: none -> 43.2 us  [local(): pl.pallas_call(functools.partial(layer_kernel, S, T, heads, (R, HD, DV, G...]
    dot_general x14 -> x0, matrix products: 27.6 us -> none  [the longest x4 9.18 us: online_step(): jnp.einsum('grmqk,kgd->grmqd', probs.astype(jnp.bfloat16), block_values,...]
    reduce_scatter x1 -> x0, waiting for transfers between devices: 24.4 us -> none  [local(): lax.psum_scatter(jnp.dot(merged, out_weight, preferred_element_type=jnp.f...]
    ppermute x7 -> x0, waiting for transfers between devices: 23.6 us -> none  [shifted(): return lax.ppermute(block, axis, route)]
    all_gather x1 -> x0, waiting for transfers between devices: 13.2 us -> none  [local(): joined = project(lax.all_gather(tokens, 'tp', axis=0, tiled=True))]
    ppermute x7 -> x0, starting transfers between devices: 9.01 us -> none  [shifted(): return lax.ppermute(block, axis, route)]
    unnamed x32 -> x6, local copies, waits for them, and re-layouts: 5.48 us -> 9.52 us
    another operation x4 -> x0, other arithmetic: 3.97 us -> none
  transfers between devices with their start and end apart: 9 -> 0, of which waited for: 7 -> 0; matrix products, arithmetic and copies ran while one was open for 13% -> 0% of each run, Pallas kernels for 0% -> 0%
where the time goes in v1:
time: 53.6 us; the launch traced here: 53.4 us
  Pallas kernels  43.2 us (81%)
  local copies, waits for them, and re-layouts  9.52 us (18%)
  between operations  0.65 us (1%)
    pallas_call x1, Pallas kernels, local(): pl.pallas_call(functools.partial(layer_kernel, S, T, heads, (R, HD, DV, G...  43.2 us
    unnamed x6, local copies, waits for them, and re-layouts  9.52 us

profile of v1, /device:TPU:28, one launch (start us, length us, event | category | flops | bytes accessed | tf_op | source)
XLA Modules:
  0.0 53.4 jit_solution(1237335492635338077)
XLA Ops:
  0.6 0.0 copy-start
  0.6 3.4 %copy.17 = bf16[256,8,4,128]{3,1,2,0:T(8,128)(2,1)} copy(bf16[256,8,4,128]{3,2,1,0:T(4,128)(2,1)} %bitcast.15) | data formatting | bytes 4194304
  4.1 0.0 copy-done
  4.1 3.1 %copy.15 = bf16[256,8,2,512]{3,1,2,0:T(8,128)(2,1)} copy(bf16[256,8,2,512]{3,2,1,0:T(2,128)(2,1)S(1)} %bitcast.14) | data formatting | bytes 8388608
  7.2 43.2 %shard_map.131 = (bf16[64,2048]{1,0:T(8,128)(2,1)}, f32[2,4,256]{2,1,0:T(4,128)}) custom-call(f32[4]{0:T(128)} %lam_ref.1, bf16[64,2048]{1,0:T(8,128)(2,1)} %tokens.1, f32[1,2048]{1,0:T(1,128)} %bitcast.20, bf16[2048,512]{1,0:T(8,128)(2,1)} %bitcast.13, bf16[2048,128]{1,0:T(8,128)(2,1)} %bitcast.17, bf16[2048,128]{1,0:T(8,128)(2,1)} %bitcast.18, ...), custom_call_target="tpu_custom_call" | custom-call | tf_op jit(solution)/shard_map/pallas_call | solution.py:335
  50.4 1.7 %copy.20 = bf16[64,2048]{1,0:T(8,128)(2,1)} copy(bf16[64,2048]{1,0:T(8,128)(2,1)} %get-tuple-element.4) | data formatting | bytes 524288
  52.1 1.3 %copy.21 = f32[2,4,256]{2,1,0:T(4,128)} copy(f32[2,4,256]{2,1,0:T(4,128)} %get-tuple-element.5) | data formatting | bytes 16384
Async XLA Ops:
  0.6 3.4 %copy-start = (bf16[2048,2,512]{2,1,0:T(2,128)(2,1)S(1)}, bf16[2048,2,512]{2,1,0:T(2,128)(2,1)}, u32[]{:S(2)}) copy-start(bf16[2048,2,512]{2,1,0:T(2,128)(2,1)} %param.22) | copy-start | bytes 12582916

commit v2 on v1

--- a/solution.py
+++ b/solution.py
@@ -19,9 +19,9 @@
     S, T, heads, dims,
     lam_ref, tokens, gain_ref, wq_h, wk_h, wv_h, hgain_ref, wp_h, mix_h, pscale_ref, wg_h, wo_h,
     out_ref, lse_ref,
-    tok, nrm, wkv, wq, wp, wg, wmix, wo, kvb, qt, acc, m_ref, l_ref, pool, gates, rim_out, rim_in,
+    tok, nrm, wkv, wq4, wq, wp, wg, x2, wmix, wo, kvb, qt, acc, m_ref, l_ref, pool, gates, rim_out, rim_in,
     merged, part_remote, part_near, got_pair, got_near, sum_out, got_sum, keep,
-    load_sem, tsend, trecv, ksend, krecv, rsem, psend, precv, ssend, srecv,
+    load_sem, tsend, trecv, asend, ksend, krecv, rsem, psend, precv, ssend, srecv,
 ):
     R, HD, DV, GW, D = dims
     A = T // 2
@@ -44,20 +44,32 @@
         pltpu.make_async_copy(tokens, tok.at[slot(t)], load_sem.at[0]),
         pltpu.make_async_copy(wk_h, wkv.at[:, pl.ds(0, 2 * HD)], load_sem.at[1]),
         pltpu.make_async_copy(wv_h, wkv.at[:, pl.ds(2 * HD, DV)], load_sem.at[2]),
-        pltpu.make_async_copy(wq_h, wq, load_sem.at[3]),
+        pltpu.make_async_copy(wq_h, wq4, load_sem.at[3]),
         pltpu.make_async_copy(wp_h, wp, load_sem.at[4]),
-        pltpu.make_async_copy(wg_h, wg, load_sem.at[5]),
-        pltpu.make_async_copy(mix_h, wmix, load_sem.at[6]),
-        pltpu.make_async_copy(wo_h, wo, load_sem.at[7]),
+        pltpu.make_async_copy(mix_h, wmix, load_sem.at[5]),
+        pltpu.make_async_copy(wo_h, wo, load_sem.at[6]),
     ]
-    for load in loads:
+    gate_loads = [
+        pltpu.make_async_copy(wg_h.at[:, c], wg.at[c], load_sem.at[7 + c]) for c in range(GW // 128)
+    ]
+    for load in loads[:4] + gate_loads + loads[4:]:
         load.start()
 
     barrier = pltpu.get_barrier_semaphore()
     count = T - 1
     for d in range(1, T):
         pl.semaphore_signal(barrier, inc=1, device_id={"tp": (t + d) % T}, device_id_type=MESH)
-    for d in (1, -1, 2, -2):
+
+    def greet(zz, carry):
+        @pl.when(zz != z)
+        def _():
+            pl.semaphore_signal(barrier, inc=1, device_id={"sp": 2 * zz + y}, device_id_type=MESH)
+
+        return carry
+
+    lax.fori_loop(0, S // 2, greet, 0)
+    count = count + S // 2 - 1
+    for d in (1, -1):
         ok = jnp.logical_and(s + d >= 0, s + d < S)
 
         @pl.when(ok)
@@ -107,11 +119,49 @@
         def _():
             kv_copy(s, p, 1, mate_s).start()
 
+    def direct_copy(d):
+        return pltpu.make_async_remote_copy(
+            src_ref=kvb.at[s, a], dst_ref=kvb.at[s, a],
+            send_sem=asend.at[d], recv_sem=krecv.at[s * A + a],
+            device_id={"sp": s + 2 * d}, device_id_type=MESH)
+
+    def send_direct(d, carry):
+        direct_copy(d).start()
+        return carry
+
+    far_steps = S // 2 - z
+
+    def gate_half(p):
+        at = pl.ds(pl.multiple_of(p * HALF, HALF), HALF)
+        er = lax.broadcasted_iota(jnp.int32, (128, 512), 0)
+        ec = lax.broadcasted_iota(jnp.int32, (128, 512), 1)
+        spread = jnp.where(ec == 2 * er + jnp.where(ec >= 256, 257, 0), 1.0, 0.0).astype(BF16)
+        for k in range(D // 128):
+            both = jnp.dot(nrm[at, k * 128:(k + 1) * 128], spread, preferred_element_type=F32).astype(BF16)
+            x2[:HALF, k * 256:(k + 1) * 256] = both[:, :256]
+            x2[HALF:, k * 256:(k + 1) * 256] = both[:, 256:]
+        rows_of = wg.reshape(GW // 128, 2 * D, 128)
+        for c in range(0, GW // 128, 2):
+            w = jnp.concatenate([rows_of[c], rows_of[c + 1]], axis=1)
+            r = jnp.dot(x2[...], w, preferred_element_type=F32).astype(BF16)
+            gates[at, c * 128:c * 128 + 256] = r[:HALF]
+            gates[at, GW + c * 128:GW + c * 128 + 256] = r[HALF:]
+
     tok_copy(mate_t, 0, mate_t).wait_recv()
     loads[1].wait()
     loads[2].wait()
     project_half(a)
-    send_half(a)
+    lax.fori_loop(1, far_steps, send_direct, 0)
+
+    @pl.when(y == 0)
+    def _():
+        kv_copy(s, a, 1, mate_s).start()
+
+    loads[3].wait()
+    wq[...] = wq4[...].reshape(D, heads * 2 * HD)
+    for load in gate_loads:
+        load.wait()
+    gate_half(a)
     for i in range(1, A):
         far = (a + i) % A
         tok_copy(2 * far + b, 0, mate_t).wait_recv()
@@ -124,7 +174,14 @@
         project_half(far)
         send_half(far)
 
-    loads[3].wait()
+    def pass_near(k, carry):
+        j = 2 * (z - k) + y
+        kv_copy(j, a, 0, mate_s).wait_recv()
+        kv_copy(j, a, 1, mate_s).start()
+        return carry
+
+    lax.fori_loop(1, z + 1, pass_near, 0)
+
     lane = lax.broadcasted_iota(jnp.int32, (rows, 2 * HD), 1)
     qscale = HD ** -0.5
     for h in range(heads):
@@ -147,8 +204,7 @@
     l_ref[...] = jnp.zeros_like(l_ref)
     acc[...] = jnp.zeros_like(acc)
 
-    def attend(j, masked):
-        blk = kvb[j].reshape(rows, 2 * HD + DV)
+    def attend(blk, masked):
         keys = blk[:, :2 * HD]
         vt = blk[:, 2 * HD:].astype(F32).T.astype(BF16)
         if masked:
@@ -175,11 +231,18 @@
     def _():
         rim_copy(s + 1).start()
 
-    attend(s, True)
+    def whole(j):
+        return kvb[j].reshape(rows, 2 * HD + DV)
+
+    def pair(zz, p):
+        return jnp.concatenate([kvb[2 * zz, p], kvb[2 * zz + 1, p]], axis=0)
+
+    attend(whole(s), True)
 
     def chain(k, carry):
         j = 2 * (z - k) + y
-        for p in range(A):
+        for i in range(1, A):
+            p = (a + i) % A
             kv_copy(j, p, 0, mate_s).wait_recv()
 
             @pl.when(has_next)
@@ -187,20 +250,26 @@
                 kv_copy(j, p, 0, s + 2).start()
 
             kv_copy(j, p, 1, mate_s).start()
-        attend(j, False)
+        kv_copy(2 * (z - k) + 1 - y, a, 0, mate_s).wait_recv()
+        attend(pair(z - k, a), False)
         return carry
 
     lax.fori_loop(1, z + 1, chain, 0)
 
-    loads[5].wait()
-    for c0 in range(0, 2 * GW, COLS):
-        gates[:, c0:c0 + COLS] = jnp.dot(nrm[...], wg[:, c0:c0 + COLS], preferred_element_type=F32).astype(BF16)
+    @pl.when(y == 1)
+    def _():
+        for p in range(A):
+            kv_copy(s - 1, p, 0, mate_s).wait_recv()
+        attend(whole(s - 1), False)
+
+    for i in range(1, A):
+        gate_half((a + i) % A)
 
     def mates(k, carry):
-        j = 2 * (z - k) + 1 - y
-        for p in range(A):
-            kv_copy(j, p, 0, mate_s).wait_recv()
-        attend(j, False)
+        for i in range(1, A):
+            p = (a + i) % A
+            kv_copy(2 * (z - k) + 1 - y, p, 0, mate_s).wait_recv()
+            attend(pair(z - k, p), False)
         return carry
 
     @pl.when(s > 0)
@@ -223,12 +292,12 @@
     total = jnp.dot(band, pool[...], preferred_element_type=F32) + jnp.dot(
         band2, rim_in[...], preferred_element_type=F32)
     pooled = (total / counts - pool[...].astype(F32)).astype(BF16)
-    loads[6].wait()
+    loads[5].wait()
     pmixed = jnp.dot(pooled, wmix[...], preferred_element_type=F32) * pscale_ref[...]
     keep_pool = jax.nn.sigmoid(gates[:, GW:].astype(F32)) * pmixed
     keep[...] = keep_pool
 
-    lax.fori_loop(1 - y, z + 1, mates, 0)
+    lax.fori_loop(1, z + 1, mates, 0)
 
     for h in range(heads):
         c1 = slice(h * QC, h * QC + rows)
@@ -243,7 +312,7 @@
         hs = slice(h * DV, (h + 1) * DV)
         merged[:, hs] = (jax.nn.sigmoid(gates[:, hs].astype(F32)) * att + keep[:, hs]).astype(BF16)
 
-    loads[7].wait()
+    loads[6].wait()
 
     def product(i):
         return jnp.dot(merged[slot(i)], wo[...], preferred_element_type=F32)
@@ -294,7 +363,7 @@
     def drain(k, carry):
         j = 2 * (z - k) + y
         for p in range(A):
-            @pl.when(has_next)
+            @pl.when(jnp.logical_and(has_next, p != a))
             def _():
                 kv_copy(j, p, 0, s + 2).wait_send()
 
@@ -304,10 +373,21 @@
         return carry
 
     lax.fori_loop(0, z + 1, drain, 0)
+
+    def drain_direct(d, carry):
+        direct_copy(d).wait_send()
+        return carry
+
+    lax.fori_loop(1, far_steps, drain_direct, 0)
     near_copy.wait_send()
     for i in range(1, A):
         pair_copy(i).wait_send()
         sum_copy(i).wait_send()
+
+
+def hand_over(out_in, sums_in, out_ref, sums_ref):
+    out_ref[...] = out_in[...]
+    sums_ref[...] = sums_in[...]
 
 
 def local(
@@ -332,7 +412,7 @@
     smem = pl.BlockSpec(memory_space=pltpu.SMEM)
     dma = pltpu.SemaphoreType.DMA
     V = pltpu.VMEM
-    return pl.pallas_call(
+    out, sums = pl.pallas_call(
         functools.partial(layer_kernel, S, T, heads, (R, HD, DV, GW, D)),
         out_shape=(
             jax.ShapeDtypeStruct((R, D), BF16),
@@ -342,24 +422,32 @@
         out_specs=(vmem, vmem),
         scratch_shapes=[
             V((rows, D), BF16), V((rows, D), BF16), V((D, kv_width), BF16),
-            V((D, heads * 2 * HD), BF16), V((D, GW), BF16), V((D, 2 * GW), BF16),
+            V((D, heads, 2 * HD), BF16), V((D, heads * 2 * HD), BF16), V((D, GW), BF16),
+            V((GW // 128, D, 2, 128), BF16), V((4 * R, 2 * D), BF16),
             V((GW, GW), BF16), V((heads * DV, D), BF16),
             V((S, A, 2 * R, kv_width), BF16), V((2 * HD, columns), BF16), V((DV, columns), F32),
             V((1, columns), F32), V((1, columns), F32), V((rows, GW), BF16), V((rows, 2 * GW), BF16),
             V((WINDOW, GW), BF16), V((WINDOW, GW), BF16), V((rows, GW), BF16),
             V((A - 1, R, D), BF16), V((R, D), BF16), V((A - 1, R, D), BF16), V((R, D), BF16),
             V((A - 1, R, D), BF16), V((A - 1, R, D), BF16), V((rows, GW), F32),
-            dma((8,)), dma((2 * A,)), dma((T,)), dma((S * A * 2,)), dma((S * A,)), dma((2,)),
+            dma((7 + GW // 128,)), dma((2 * A,)), dma((T,)), dma((S // 2,)), dma((S * A * 2,)), dma((S * A,)), dma((2,)),
             dma((A,)), dma((A,)), dma((A,)), dma((A,)),
         ],
         compiler_params=pltpu.CompilerParams(
             collective_id=0, has_side_effects=True, vmem_limit_bytes=60 * 1024 * 1024),
     )(
-        mix_lambda, tokens, norm_gain.reshape(1, D), query_weight.reshape(D, -1),
+        mix_lambda, tokens, norm_gain.reshape(1, D), query_weight,
         key_weight.reshape(D, -1), value_weight.reshape(D, -1), head_gain.reshape(1, DV),
         pool_weight.reshape(D, -1), pool_mix.reshape(GW, GW), pool_scale,
-        gate_weight.reshape(D, -1), out_weight,
+        gate_weight.reshape(D, 2, GW // 128, 128).transpose(0, 2, 1, 3), out_weight,
     )
+    return pl.pallas_call(
+        hand_over,
+        out_shape=(jax.ShapeDtypeStruct(out.shape, BF16), jax.ShapeDtypeStruct(sums.shape, F32)),
+        in_specs=[vmem, vmem],
+        out_specs=(vmem, vmem),
+        compiler_params=pltpu.CompilerParams(vmem_limit_bytes=4 * 1024 * 1024),
+    )(out, sums)
 
 
 def solution(mesh):

time: 53.6 us -> 47.2 us (0.88)
  local copies, waits for them, and re-layouts: 9.52 us -> 1.64 us
  Pallas kernels: 43.2 us -> 44.4 us
    unnamed x6 -> x4, local copies, waits for them, and re-layouts: 9.52 us -> 1.64 us
    pallas_call x0 -> x1, Pallas kernels: none -> 0.72 us  [local(): pl.pallas_call(hand_over, out_shape=(jax.ShapeDtypeStruct(out.shape, BF16...]
where the time goes in v2:
time: 47.2 us; the launch traced here: 46.7 us
  Pallas kernels  44.4 us (94%)
  local copies, waits for them, and re-layouts  1.64 us (3%)
  between operations  0.65 us (1%)
    pallas_call x1, Pallas kernels, local(): pl.pallas_call(functools.partial(layer_kernel, S, T, heads, (R, HD, DV, G...  43.7 us
    unnamed x4, local copies, waits for them, and re-layouts  1.64 us

profile of v2, /device:TPU:28, one launch (start us, length us, event | category | flops | bytes accessed | tf_op | source)
XLA Modules:
  0.0 46.7 jit_solution(13016431499089488548)
XLA Ops:
  0.6 43.7 %shard_map.131 = (bf16[64,2048]{1,0:T(8,128)(2,1)}, f32[2,4,256]{2,1,0:T(4,128)}) custom-call(f32[4]{0:T(128)} %lam_ref.1, bf16[64,2048]{1,0:T(8,128)(2,1)} %tokens.1, f32[1,2048]{1,0:T(1,128)} %bitcast.14, bf16[2048,4,128]{2,1,0:T(4,128)(2,1)} %wq_h.1, bf16[2048,128]{1,0:T(8,128)(2,1)} %bitcast.11, bf16[2048,128]{1,0:T(8,128)(2,1)} %bitcast.12, ...), custom_call_target="tpu_custom_call" | custom-call | tf_op jit(solution)/shard_map/pallas_call | solution.py:415
  44.4 0.0 copy-start
  44.4 0.9 %copy-done = bf16[64,2048]{1,0:T(8,128)(2,1)S(1)} copy-done((bf16[64,2048]{1,0:T(8,128)(2,1)S(1)}, bf16[64,2048]{1,0:T(8,128)(2,1)}, u32[]{:S(2)}) %copy-start) | copy-done | bytes 262168
  45.3 0.0 copy-start.1
  45.3 0.7 %copy-done.1 = f32[2,4,256]{2,1,0:T(4,128)S(1)} copy-done((f32[2,4,256]{2,1,0:T(4,128)S(1)}, f32[2,4,256]{2,1,0:T(4,128)}, u32[]{:S(2)}) %copy-start.1) | copy-done | bytes 8216
  46.0 0.7 %shard_map.132 = (bf16[64,2048]{1,0:T(8,128)(2,1)}, f32[2,4,256]{2,1,0:T(4,128)}) custom-call(bf16[64,2048]{1,0:T(8,128)(2,1)S(1)} %copy-done, f32[2,4,256]{2,1,0:T(4,128)S(1)} %copy-done.1), custom_call_target="tpu_custom_call" | custom-call | tf_op jit(solution)/shard_map/pallas_call | solution.py:444
Async XLA Ops:
  44.4 1.0 %copy-start = (bf16[64,2048]{1,0:T(8,128)(2,1)S(1)}, bf16[64,2048]{1,0:T(8,128)(2,1)}, u32[]{:S(2)}) copy-start(bf16[64,2048]{1,0:T(8,128)(2,1)} %get-tuple-element.4.out_in) | copy-start | bytes 786436
  45.3 0.7 %copy-start.1 = (f32[2,4,256]{2,1,0:T(4,128)S(1)}, f32[2,4,256]{2,1,0:T(4,128)}, u32[]{:S(2)}) copy-start(f32[2,4,256]{2,1,0:T(4,128)} %get-tuple-element.5.sums_in) | copy-start | bytes 24580

commit v3 on v2

--- a/solution.py
+++ b/solution.py
@@ -159,9 +159,6 @@
 
     loads[3].wait()
     wq[...] = wq4[...].reshape(D, heads * 2 * HD)
-    for load in gate_loads:
-        load.wait()
-    gate_half(a)
     for i in range(1, A):
         far = (a + i) % A
         tok_copy(2 * far + b, 0, mate_t).wait_recv()
@@ -252,8 +249,15 @@
             kv_copy(j, p, 1, mate_s).start()
         kv_copy(2 * (z - k) + 1 - y, a, 0, mate_s).wait_recv()
         attend(pair(z - k, a), False)
-        return carry
-
+
+        @pl.when(k <= A)
+        def _():
+            gate_half((a + k - 1) % A)
+
+        return carry
+
+    for load in gate_loads:
+        load.wait()
     lax.fori_loop(1, z + 1, chain, 0)
 
     @pl.when(y == 1)
@@ -262,8 +266,11 @@
             kv_copy(s - 1, p, 0, mate_s).wait_recv()
         attend(whole(s - 1), False)
 
-    for i in range(1, A):
-        gate_half((a + i) % A)
+    def late_gates(k, carry):
+        gate_half((a + k - 1) % A)
+        return carry
+
+    lax.fori_loop(jnp.minimum(z, A) + 1, A + 1, late_gates, 0)
 
     def mates(k, carry):
         for i in range(1, A):
@@ -385,9 +392,13 @@
         sum_copy(i).wait_send()
 
 
-def hand_over(out_in, sums_in, out_ref, sums_ref):
-    out_ref[...] = out_in[...]
-    sums_ref[...] = sums_in[...]
+def hand_over(out_in, sums_in, out_ref, sums_ref, sem):
+    first = pltpu.make_async_copy(out_in, out_ref, sem.at[0])
+    second = pltpu.make_async_copy(sums_in, sums_ref, sem.at[1])
+    first.start()
+    second.start()
+    first.wait()
+    second.wait()
 
 
 def local(
@@ -444,8 +455,9 @@
     return pl.pallas_call(
         hand_over,
         out_shape=(jax.ShapeDtypeStruct(out.shape, BF16), jax.ShapeDtypeStruct(sums.shape, F32)),
-        in_specs=[vmem, vmem],
+        in_specs=[hbm, hbm],
         out_specs=(vmem, vmem),
+        scratch_shapes=[dma((2,))],
         compiler_params=pltpu.CompilerParams(vmem_limit_bytes=4 * 1024 * 1024),
     )(out, sums)
 

time: 47.2 us -> 47.8 us (1.013)
  Pallas kernels: 44.4 us -> 45.2 us
    pallas_call x1, Pallas kernels: 43.7 us -> 44.4 us  [local(): pl.pallas_call(functools.partial(layer_kernel, S, T, heads, (R, HD, DV, G...]
where the time goes in v3:
time: 47.8 us; the launch traced here: 47.6 us
  Pallas kernels  45.2 us (95%)
  local copies, waits for them, and re-layouts  1.64 us (3%)
  between operations  0.81 us (2%)
    pallas_call x1, Pallas kernels, local(): pl.pallas_call(functools.partial(layer_kernel, S, T, heads, (R, HD, DV, G...  44.4 us
    unnamed x4, local copies, waits for them, and re-layouts  1.64 us

profile of v3, /device:TPU:28, one launch (start us, length us, event | category | flops | bytes accessed | tf_op | source)
XLA Modules:
  0.0 47.6 jit_solution(14943213961757800183)
XLA Ops:
  0.6 44.4 %shard_map.131 = (bf16[64,2048]{1,0:T(8,128)(2,1)}, f32[2,4,256]{2,1,0:T(4,128)}) custom-call(f32[4]{0:T(128)} %lam_ref.1, bf16[64,2048]{1,0:T(8,128)(2,1)} %tokens.1, f32[1,2048]{1,0:T(1,128)} %bitcast.14, bf16[2048,4,128]{2,1,0:T(4,128)(2,1)} %wq_h.1, bf16[2048,128]{1,0:T(8,128)(2,1)} %bitcast.11, bf16[2048,128]{1,0:T(8,128)(2,1)} %bitcast.12, ...), custom_call_target="tpu_custom_call" | custom-call | tf_op jit(solution)/shard_map/pallas_call | solution.py:426
  45.1 0.0 copy-start
  45.1 0.9 %copy-done = bf16[64,2048]{1,0:T(8,128)(2,1)S(1)} copy-done((bf16[64,2048]{1,0:T(8,128)(2,1)S(1)}, bf16[64,2048]{1,0:T(8,128)(2,1)}, u32[]{:S(2)}) %copy-start) | copy-done | bytes 262168
  46.0 0.0 copy-start.1
  46.0 0.7 %copy-done.1 = f32[2,4,256]{2,1,0:T(4,128)S(1)} copy-done((f32[2,4,256]{2,1,0:T(4,128)S(1)}, f32[2,4,256]{2,1,0:T(4,128)}, u32[]{:S(2)}) %copy-start.1) | copy-done | bytes 8216
  46.7 0.7 %shard_map.132 = (bf16[64,2048]{1,0:T(8,128)(2,1)}, f32[2,4,256]{2,1,0:T(4,128)}) custom-call(bf16[64,2048]{1,0:T(8,128)(2,1)S(1)} %copy-done, f32[2,4,256]{2,1,0:T(4,128)S(1)} %copy-done.1), custom_call_target="tpu_custom_call" | custom-call | tf_op jit(solution)/shard_map/pallas_call | solution.py:455
Async XLA Ops:
  45.1 1.0 %copy-start = (bf16[64,2048]{1,0:T(8,128)(2,1)S(1)}, bf16[64,2048]{1,0:T(8,128)(2,1)}, u32[]{:S(2)}) copy-start(bf16[64,2048]{1,0:T(8,128)(2,1)} %get-tuple-element.4.out_in) | copy-start | bytes 786436
  46.0 0.7 %copy-start.1 = (f32[2,4,256]{2,1,0:T(4,128)S(1)}, f32[2,4,256]{2,1,0:T(4,128)}, u32[]{:S(2)}) copy-start(f32[2,4,256]{2,1,0:T(4,128)} %get-tuple-element.5.sums_in) | copy-start | bytes 24580
